TPU v7x, 32 devices: a whole 2x2x4 slice. The times are simulated.
32 devices in a mesh: ep: 16 (over z, x, core), tp: 2 (over y).
Axes of the slice: x: 2, y: 2, z: 4, core: 2. Of those that a mesh axis runs over, the one named last changes fastest.
Arguments:
- tokens: bfloat16 [256, 1024], P('ep'), may hold values from -6 to 6
- state: float32 [256, 16, 64, 64], P('ep', 'tp'), may hold values from -6 to 6
- w_recep: bfloat16 [1024, 1024], P(None, 'tp'), may hold values from -0.1875 to 0.1875
- w_key: bfloat16 [1024, 1024], P(None, 'tp'), may hold values from -0.1875 to 0.1875
- w_value: bfloat16 [1024, 1024], P(None, 'tp'), may hold values from -0.1875 to 0.1875
- w_out: bfloat16 [1024, 1024], P('tp'), may hold values from -0.1875 to 0.1875
- decay_base: float32 [1024], P('tp'), may hold values from -5 to 1
- decay_down: bfloat16 [1024, 64], replicated, may hold values from -0.1875 to 0.1875
- decay_up: bfloat16 [64, 1024], P(None, 'tp'), may hold values from -1 to 1
- rate_base: float32 [1024], P('tp'), may hold values from -4 to 4
- rate_down: bfloat16 [1024, 64], replicated, may hold values from -0.1875 to 0.1875
- rate_up: bfloat16 [64, 1024], P(None, 'tp'), may hold values from -1 to 1
- head_gain: float32 [1024], P('tp'), may hold values from 0.1 to 1.9
- first_gain: float32 [1024], replicated, may hold values from 0.2 to 4.8
- expert_gate: bfloat16 [16, 1024, 1408], P('ep', None, 'tp'), may hold values from -0.1875 to 0.1875
- expert_up: bfloat16 [16, 1024, 1408], P('ep', None, 'tp'), may hold values from -0.1875 to 0.1875
- expert_down: bfloat16 [16, 1408, 1024], P('ep', 'tp'), may hold values from -0.078125 to 0.078125
- dense_gate: bfloat16 [2816, 1024], P('ep'), may hold values from -0.1875 to 0.1875
- dense_up: bfloat16 [2816, 1024], P('ep'), may hold values from -0.1875 to 0.1875
- dense_down: bfloat16 [2816, 1024], P('ep', 'tp'), may hold values from -0.21875 to 0.21875
- branch_gate: bfloat16 [1024], replicated, may hold values from -0.1875 to 0.1875
- second_gain: float32 [1024], P('tp'), may hold values from 0.1 to 1.9
- routes: int32 [256, 2], P('ep'), may hold values from 0 to 3, all different within a row; in each aligned block of 16 rows (0 to 15, 16 to 31, ...) at most 16 rows name the same one
- route_weights: float32 [256, 2], P('ep'), may hold values from 0.2 to 1
Outputs:
- layer_output: bfloat16 [256, 1024], P('ep', 'tp')
Inputs may be any that keep to these rules, and one draw needn't show every extreme that they name: `routes`: each row names 2 different experts. In each aligned block of 16 rows no expert is named by more than 16 rows, a bound that some block reaches.
All inputs are finite; a program needn't handle non-finite values.
Results may differ from a plain program's by a relative error of at most 0.018.
Values may be sent and summed in bfloat16 or wider, within the bound.
A program may use at most 64 MiB of HBM per device.

v0:
```python
import jax
import jax.numpy as jnp
from jax import lax
from jax.sharding import PartitionSpec as P

SPLIT = 4
residual_scale = 1.4142135623730951
norm_epsilon = 1e-05
head_epsilon = 0.00064
key_epsilon = 1e-06


def time_mixer(
    tokens,
    state,
    w_recep,
    w_key,
    w_value,
    w_out,
    decay_base,
    decay_down,
    decay_up,
    rate_base,
    rate_down,
    rate_up,
    head_gain,
):
    row_count = tokens.shape[0]
    head_count = state.shape[1]
    head_size = state.shape[3]
    recep = jnp.dot(tokens, w_recep, preferred_element_type=jnp.float32).reshape(
        row_count, head_count, head_size
    )
    key_vecs = jnp.dot(tokens, w_key, preferred_element_type=jnp.float32).reshape(
        row_count, head_count, head_size
    )
    value_vecs = jnp.dot(tokens, w_value, preferred_element_type=jnp.float32).reshape(
        row_count, head_count, head_size
    )
    decay_low = jnp.tanh(jnp.dot(tokens, decay_down, preferred_element_type=jnp.float32)).astype(
        jnp.bfloat16
    )
    decay_pre = decay_base + jnp.dot(decay_low, decay_up, preferred_element_type=jnp.float32)
    log_rate = -jax.nn.softplus(-decay_pre) - 0.5
    decay = jnp.exp(-jnp.exp(log_rate)).reshape(row_count, head_count, head_size)
    rate_low = jnp.dot(tokens, rate_down, preferred_element_type=jnp.float32).astype(jnp.bfloat16)
    in_rate = jax.nn.sigmoid(
        rate_base + jnp.dot(rate_low, rate_up, preferred_element_type=jnp.float32)
    ).reshape(row_count, head_count, head_size)
    unit_keys = key_vecs * lax.rsqrt(jnp.sum(key_vecs * key_vecs, -1, keepdims=True) + key_epsilon)
    removed = jnp.einsum("bhij,bhj->bhi", state, -unit_keys)
    updated = (
        state * decay[:, :, None, :]
        + removed[..., None] * (unit_keys * in_rate)[:, :, None, :]
        + value_vecs[..., None] * key_vecs[:, :, None, :]
    )
    read_out = jnp.einsum("bhij,bhj->bhi", updated, recep)
    centre = jnp.mean(read_out, -1, keepdims=True)
    spread = jnp.mean(jnp.square(read_out - centre), -1, keepdims=True)
    normed = ((read_out - centre) * lax.rsqrt(spread + head_epsilon)).reshape(
        row_count, head_count * head_size
    ) * head_gain
    return jnp.dot(normed.astype(jnp.bfloat16), w_out, preferred_element_type=jnp.float32)


def first_norm(values, gain):
    centre = jnp.mean(values, -1, keepdims=True)
    spread = jnp.mean(jnp.square(values - centre), -1, keepdims=True)
    return ((values - centre) * lax.rsqrt(spread + norm_epsilon) * gain).astype(jnp.bfloat16)


def route_tables(routes, route_weights, experts, capacity):
    expert_hits = (
        routes[:, :, None] == jnp.arange(experts, dtype=jnp.int32)[None, None, :]
    ).astype(jnp.int32)
    row_hits = jnp.sum(expert_hits, 1, dtype=jnp.int32)
    earlier = jnp.cumsum(row_hits, 0, dtype=jnp.int32) - row_hits
    slot_index = jnp.sum(earlier[:, None, :] * expert_hits, 2, dtype=jnp.int32)
    target = routes * capacity + slot_index
    places = jnp.arange(experts * capacity, dtype=jnp.int32)
    slot_match = target[:, :, None] == places[None, None, :]
    dispatch_tokens = jnp.any(slot_match, 1).astype(jnp.bfloat16)
    combine_experts = jnp.sum(jnp.where(slot_match, route_weights[:, :, None], 0.0), 1)
    return (dispatch_tokens, combine_experts)


def shards(
    tokens,
    state,
    w_recep,
    w_key,
    w_value,
    w_out,
    decay_base,
    decay_down,
    decay_up,
    rate_base,
    rate_down,
    rate_up,
    head_gain,
    first_gain,
    expert_gate,
    expert_up,
    expert_down,
    dense_gate,
    dense_up,
    dense_down,
    branch_gate,
    second_gain,
    routes,
    route_weights,
):
    row_count = tokens.shape[0]
    model_width = tokens.shape[1]
    quarter = w_recep.shape[1]
    tp_index = lax.axis_index("tp")
    partial_mix = time_mixer(
        tokens,
        state,
        w_recep,
        w_key,
        w_value,
        w_out,
        decay_base,
        decay_down,
        decay_up,
        rate_base,
        rate_down,
        rate_up,
        head_gain,
    )
    mixed = lax.psum(partial_mix, "tp")
    x_mid = first_norm(residual_scale * tokens.astype(jnp.float32) + mixed, first_gain)
    own_columns = lax.dynamic_slice_in_dim(x_mid, tp_index * quarter, quarter, 1)
    experts = lax.axis_size("ep") // SPLIT
    capacity = min(row_count, max(2, 2 * row_count * routes.shape[1] // experts))
    dispatch_tokens, combine_experts = route_tables(routes, route_weights, experts, capacity)
    packed_rows = lax.dot_general(
        dispatch_tokens, x_mid, (((0,), (0,)), ((), ())), preferred_element_type=jnp.float32
    ).astype(jnp.bfloat16)
    outgoing = jnp.repeat(packed_rows.reshape(experts, capacity, x_mid.shape[1]), SPLIT, axis=0)
    arrived = lax.all_to_all(outgoing, "ep", split_axis=0, concat_axis=0, tiled=True)
    sources = arrived.shape[0]
    slot_count = arrived.shape[1]
    flat_rows = arrived.reshape(sources * slot_count, model_width)
    gate_pre = jnp.dot(flat_rows, expert_gate[0], preferred_element_type=jnp.float32)
    up_pre = jnp.dot(flat_rows, expert_up[0], preferred_element_type=jnp.float32)
    hidden = (jax.nn.silu(gate_pre) * up_pre).astype(jnp.bfloat16)
    partial_out = jnp.dot(hidden, expert_down[0], preferred_element_type=jnp.float32).reshape(
        sources, slot_count, model_width
    )
    summed = lax.psum_scatter(
        partial_out.astype(jnp.bfloat16), "tp", scatter_dimension=2, tiled=True
    ).astype(jnp.float32)
    returned = lax.all_to_all(
        summed.astype(jnp.bfloat16), "ep", split_axis=0, concat_axis=0, tiled=True
    ).astype(summed.dtype)
    expert_out = jnp.sum(returned.reshape(experts, SPLIT, capacity, quarter), 1).reshape(
        experts * capacity, quarter
    )
    routed_part = jnp.dot(
        combine_experts,
        expert_out,
        precision=lax.Precision.HIGHEST,
        preferred_element_type=jnp.float32,
    )
    branch = jax.nn.sigmoid(jnp.dot(x_mid, branch_gate, preferred_element_type=jnp.float32))
    shard_rows = lax.all_gather(x_mid, "ep", axis=0, tiled=True)
    gate_pre = lax.dot_general(
        shard_rows, dense_gate, (((1,), (1,)), ((), ())), preferred_element_type=jnp.float32
    )
    up_pre = lax.dot_general(
        shard_rows, dense_up, (((1,), (1,)), ((), ())), preferred_element_type=jnp.float32
    )
    dense_hidden = (jax.nn.silu(gate_pre) * up_pre).astype(jnp.bfloat16)
    dense_part = lax.psum_scatter(
        jnp.dot(dense_hidden, dense_down, preferred_element_type=jnp.float32),
        "ep",
        scatter_dimension=0,
        tiled=True,
    )
    second_sum = (
        residual_scale * own_columns.astype(jnp.float32)
        + routed_part
        + branch[:, None] * dense_part
    )
    row_sums, square_sums = lax.psum(
        (jnp.sum(second_sum, 1), jnp.sum(second_sum * second_sum, 1)), "tp"
    )
    average = row_sums / model_width
    spread = square_sums / model_width - average * average
    return (
        (second_sum - average[:, None]) * lax.rsqrt(spread + norm_epsilon)[:, None] * second_gain
    ).astype(jnp.bfloat16)


def solution(mesh):
    return jax.shard_map(
        shards,
        mesh=mesh,
        in_specs=(
            P("ep", None),
            P("ep", "tp", None, None),
            P(None, "tp"),
            P(None, "tp"),
            P(None, "tp"),
            P("tp", None),
            P("tp"),
            P(),
            P(None, "tp"),
            P("tp"),
            P(),
            P(None, "tp"),
            P("tp"),
            P(),
            P("ep", None, "tp"),
            P("ep", None, "tp"),
            P("ep", "tp", None),
            P("ep", None),
            P("ep", None),
            P("ep", "tp"),
            P(),
            P("tp"),
            P("ep", None),
            P("ep", None),
        ),
        out_specs=P("ep", "tp"),
        check_vma=False,
    )
```

profile of v0, /device:TPU:0, one launch (start us, length us, event | category | flops | bytes accessed | tf_op | source)
XLA Modules:
  0.0 162.2 jit_solution(11377209794120408051)
XLA Ops:
  6.5 1.6 fusion.56
  8.1 0.1 reshape.96
  8.2 0.1 multiply_reduce_fusion.2
  8.3 1.2 fusion.32
  9.6 0.1 reshape.97
  9.6 1.5 fusion.59
  11.1 0.1 reshape.110
  11.2 1.3 fusion.49
  12.5 0.1 mul.167
  12.6 1.5 fusion.58
  14.0 0.1 mul.177
  14.1 0.1 multiply_negate_fusion
  14.2 3.5 %fusion.57 = f32[16,8,1,64]{3,2,1,0:T(1,128)S(1)} fusion(f32[16,8,64,1]{2,3,1,0:T(1,128)S(1)} %bitcast.81, f32[16,8,64,64]{3,2,1,0:T(8,128)} %param.25), kind=kOutput, calls=%fused_computation.85 | convolution fusion | flops 1048576 | bytes 2162688 | tf_op jit(solution)/shard_map/bhij,bhj->bhi/dot_general | solution.py:51
  17.8 0.0 copy-start.6
  17.8 2.9 %fusion = f32[16,8,1,64]{3,2,1,0:T(1,128)S(1)} fusion(f32[16,8,64,1]{2,3,1,0:T(1,128)S(1)} %bitcast.83, f32[16,8,64,64]{3,2,1,0:T(8,128)S(1)} %copy-done.1, f32[16,8,64]{2,1,0:T(8,128)S(1)} %reshape.96, f32[16,8,64]{2,1,0:T(8,128)S(1)} %mul.177, f32[16,8,64]{2,1,0:T(8,128)S(1)} %get-tuple-element.10, f32[16,8,64]{2,1,0:T(8,128)S(1)} %bitcast.82, ...), kind=kOutput, calls=%fused_computation | convolution fusion | flops 3670016 | bytes 2326528 | tf_op jit(solution)/shard_map/bhij,bhj->bhi/dot_general | solution.py:57
  20.7 0.1 reduce_sum.100
  20.8 0.2 multiply_reduce_fusion.1
  21.0 0.1 subtract_multiply_fusion
  21.1 0.1 reshape.99
  21.2 2.1 %fusion.51 = f32[16,1024]{1,0:T(8,128)} fusion(bf16[512,1024]{1,0:T(8,128)(2,1)} %param.29, f32[16,512]{1,0:T(8,128)S(1)} %reshape.99, f32[512]{0:T(512)S(1)} %copy-done.7), kind=kOutput, calls=%fused_computation.66 | convolution fusion | flops 16793600 | bytes 1148928 | tf_op jit(solution)/shard_map/dot_general | solution.py:63
  23.3 0.0 reduce-scatter.3.cloned.1.call-start
  23.4 0.1 copy.33
  23.5 0.1 copy.35
  23.6 0.1 fusion.52
  23.7 23.4 %all-reduce.3.cloned.1.call-done = f32[16,1024]{1,0:T(8,128)} async-done(((f32[16,1024]{1,0:T(8,128)}), f32[16,1024]{1,0:T(8,128)}) %all-reduce.3.cloned.1.call-update) | async-done | bytes 65552 | tf_op jit(solution)/shard_map/psum | solution.py:132
  47.2 1.1 fusion.50
  48.2 1.0 multiply_reduce_fusion
  49.3 0.9 multiply_convert_fusion
  50.2 0.2 convolution_convert_fusion
  50.5 0.1 broadcast_in_dim.12
  50.5 19.7 %all_to_all.10 = bf16[16,16,1024]{2,1,0:T(8,128)(2,1)S(1)} all-to-all(bf16[16,16,1024]{2,1,0:T(8,128)(2,1)S(1)} %bitcast.72), channel_id=1, replica_groups=mesh['ep'=16,'tp'=2] {'ep'}, dimensions={0} | all-to-all | bytes 1048576 | tf_op jit(solution)/shard_map/all_to_all | solution.py:142
  70.2 0.6 fusion.15
  70.8 0.6 fusion.23
  71.4 0.2 copy.36
  71.6 1.4 fusion.17
  73.1 0.0 reduce-scatter.5.cloned.1.call-start
  73.1 21.3 %all_gather.3 = bf16[256,1024]{1,0:T(8,128)(2,1)S(1)} all-gather(bf16[16,1024]{1,0:T(8,128)(2,1)S(1)} %multiply_convert_fusion), channel_id=1, replica_groups=mesh['ep'=16,'tp'=2] {'ep'}, dimensions={0}, use_global_device_ids=true | all-gather | bytes 557056 | tf_op jit(solution)/shard_map/all_gather | solution.py:168
  94.4 0.3 fusion.60
  94.8 1.5 fusion.27
  96.3 0.0 reduce-scatter.3.cloned.1.call-done
  96.3 3.5 %all-to-all-start.1 = ((bf16[16,16,512]{2,1,0:T(8,128)(2,1)}), bf16[16,16,512]{2,1,0:T(8,128)(2,1)S(1)}, u32[]{:S(2)}, u32[]{:S(2)}) async-start(bf16[16,16,512]{2,1,0:T(8,128)(2,1)} %reduce-scatter.3.cloned.1.call-done), calls=%async_computation.2 | async-start | bytes 524288 | tf_op jit(solution)/shard_map/all_to_all | solution.py:155
  99.9 0.1 select_reduce_fusion
  100.0 0.1 fusion.38
  100.1 9.7 %all-to-all-done.1 = bf16[16,16,512]{2,1,0:T(8,128)(2,1)S(1)} async-done(((bf16[16,16,512]{2,1,0:T(8,128)(2,1)}), bf16[16,16,512]{2,1,0:T(8,128)(2,1)S(1)}, u32[]{:S(2)}, u32[]{:S(2)}) %all-to-all-start.1) | async-done | bytes 262176 | tf_op jit(solution)/shard_map/all_to_all | solution.py:155
  109.9 39.1 %reduce-scatter.5.cloned.1.call-done = f32[16,512]{1,0:T(8,128)} async-done(((f32[256,512]{1,0:T(8,128)}), f32[16,512]{1,0:T(8,128)}) %reduce-scatter.5.cloned.1.call-update) | async-done | bytes 32784 | tf_op jit(solution)/shard_map/reduce_scatter | solution.py:176
  148.9 1.1 fusion.55
  150.0 4.9 %all-reduce = (f32[16]{0:T(128)S(1)}, f32[16]{0:T(128)S(1)}) all-reduce(f32[16]{0:T(128)S(1)} %get-tuple-element.6, f32[16]{0:T(128)S(1)} %get-tuple-element.5), channel_id=1, replica_groups=mesh['ep'=16,'tp'=2] {'tp'}, use_global_device_ids=true, to_apply=%region_17.18 | all-reduce | flops 32 | bytes 256 | tf_op jit(solution)/shard_map/psum | solution.py:187
  154.9 0.7 multiply_convert_fusion.1
  (44 shorter events, 0.3 us)
Async XLA Ops:
  6.5 65.1 %copy-start = (bf16[1,704,1024]{2,1,0:T(8,128)(2,1)S(1)}, bf16[1,704,1024]{2,1,0:T(8,128)(2,1)}, u32[]{:S(2)}) copy-start(bf16[1,704,1024]{2,1,0:T(8,128)(2,1)} %param.40) | copy-start | bytes 4325380
  6.5 40.6 %all-reduce.3.cloned.1.call-start = ((), (), s32[]{:S(2)}) async-start(), calls=%async_computation.4 | async-start | bytes 131072 | tf_op jit(solution)/shard_map/psum | solution.py:132
  14.1 3.6 %copy-start.1 = (f32[16,8,64,64]{3,2,1,0:T(8,128)S(1)}, f32[16,8,64,64]{3,2,1,0:T(8,128)}, u32[]{:S(2)}) copy-start(f32[16,8,64,64]{3,2,1,0:T(8,128)} %param.25) | copy-start | bytes 6291460
  17.7 3.5 %copy-start.7 = (f32[512]{0:T(512)S(1)}, f32[512]{0:T(512)}, u32[]{:S(2)}) copy-start(f32[512]{0:T(512)} %param.36) | copy-start | bytes 6148
  17.7 5.6 %copy-start.5 = (s32[16,2]{0,1:T(2,128)S(1)}, s32[16,2]{0,1:T(2,128)}, u32[]{:S(2)}) copy-start(s32[16,2]{0,1:T(2,128)} %param.46) | copy-start | bytes 388
  17.7 29.4 %copy-start.2 = (bf16[16,1024]{1,0:T(8,128)(2,1)S(1)}, bf16[16,1024]{1,0:T(8,128)(2,1)}, u32[]{:S(2)}) copy-start(bf16[16,1024]{1,0:T(8,128)(2,1)} %param.24) | copy-start | bytes 98308
  17.8 31.5 %copy-start.6 = (f32[1024]{0:T(1024)S(1)}, f32[1024]{0:T(1024)}, u32[]{:S(2)}) copy-start(f32[1024]{0:T(1024)} %param.37) | copy-start | bytes 12292
  17.8 52.4 %copy-start.3 = (bf16[1,1024,704]{1,2,0:T(8,128)(2,1)S(1)}, bf16[1,1024,704]{1,2,0:T(8,128)(2,1)}, u32[]{:S(2)}) copy-start(bf16[1,1024,704]{1,2,0:T(8,128)(2,1)} %param.38) | copy-start | bytes 4325380
  23.3 73.0 %reduce-scatter.3.cloned.1.call-start = ((), (), s32[]{:S(2)}) async-start(), calls=%async_computation.5 | async-start | bytes 786432 | tf_op jit(solution)/shard_map/reduce_scatter | solution.py:152
  47.2 23.6 %copy-start.11 = (bf16[1,1024,704]{1,2,0:T(8,128)(2,1)S(1)}, bf16[1,1024,704]{1,2,0:T(8,128)(2,1)}, u32[]{:S(2)}) copy-start(bf16[1,1024,704]{1,2,0:T(8,128)(2,1)} %param.39) | copy-start | bytes 4325380
  70.8 23.6 %copy-start.4 = (bf16[176,1024]{1,0:T(8,128)(2,1)S(1)}, bf16[176,1024]{1,0:T(8,128)(2,1)}, u32[]{:S(2)}) copy-start(bf16[176,1024]{1,0:T(8,128)(2,1)} %param.41) | copy-start | bytes 1081348
  70.8 23.9 %copy-start.12 = (bf16[176,1024]{1,0:T(8,128)(2,1)S(1)}, bf16[176,1024]{1,0:T(8,128)(2,1)}, u32[]{:S(2)}) copy-start(bf16[176,1024]{1,0:T(8,128)(2,1)} %param.42) | copy-start | bytes 1081348
  70.8 23.9 %copy-start.13 = (bf16[176,512]{1,0:T(8,128)(2,1)S(1)}, bf16[176,512]{1,0:T(8,128)(2,1)}, u32[]{:S(2)}) copy-start(bf16[176,512]{1,0:T(8,128)(2,1)} %param.43) | copy-start | bytes 540676
  71.4 28.4 %copy-start.8 = (bf16[1024]{0:T(1024)(128)(2,1)S(1)}, bf16[1024]{0:T(1024)(128)(2,1)}, u32[]{:S(2)}) copy-start(bf16[1024]{0:T(1024)(128)(2,1)} %param.44) | copy-start | bytes 6148
  71.4 28.4 %copy-start.10 = (f32[16,2]{0,1:T(2,128)S(1)}, f32[16,2]{0,1:T(2,128)}, u32[]{:S(2)}) copy-start(f32[16,2]{0,1:T(2,128)} %param.47) | copy-start | bytes 388
  71.6 83.3 %copy-start.9 = (f32[512]{0:T(512)S(1)}, f32[512]{0:T(512)}, u32[]{:S(2)}) copy-start(f32[512]{0:T(512)} %param.45) | copy-start | bytes 6148
  73.1 75.9 %reduce-scatter.5.cloned.1.call-start = ((), (), s32[]{:S(2)}) async-start(), calls=%async_computation.6 | async-start | bytes 557056 | tf_op jit(solution)/shard_map/reduce_scatter | solution.py:176
  96.3 13.5 %all-to-all-start.1 = ((bf16[16,16,512]{2,1,0:T(8,128)(2,1)}), bf16[16,16,512]{2,1,0:T(8,128)(2,1)S(1)}, u32[]{:S(2)}, u32[]{:S(2)}) async-start(bf16[16,16,512]{2,1,0:T(8,128)(2,1)} %reduce-scatter.3.cloned.1.call-done), calls=%async_computation.2 | async-start | bytes 524288 | tf_op jit(solution)/shard_map/all_to_all | solution.py:155
Sparse Core Ops, SparseCore 0:
  23.4 23.6 all-reduce.2
  73.2 13.2 reduce-scatter.2
  96.4 52.5 reduce-scatter.4
where the time goes:
time: 163 us; the launch traced here: 162 us
  waiting for transfers between devices  72.3 us (44%)
  blocking collectives  45.9 us (28%)
  matrix products  21.3 us (13%)
  between operations  13.4 us (8%)
  other arithmetic  4.56 us (3%)
  starting transfers between devices  3.63 us (2%)
    reduce_scatter x1, waiting for transfers between devices, shards(): lax.psum_scatter(jnp.dot(dense_hidden, dense_down, preferred_element_type...  39.1 us
    psum x1, waiting for transfers between devices, shards(): mixed = lax.psum(partial_mix, 'tp')  23.4 us
    all_gather x1, blocking collectives, shards(): shard_rows = lax.all_gather(x_mid, 'ep', axis=0, tiled=True)  21.3 us
    all_to_all x1, blocking collectives, shards(): lax.all_to_all(outgoing, 'ep', split_axis=0, concat_axis=0, tiled=True)  19.7 us
    all_to_all x1, waiting for transfers between devices, shards(): lax.all_to_all(summed.astype(jnp.bfloat16), 'ep', split_axis=0, concat_ax...  9.73 us
    psum x1, blocking collectives, shards(): lax.psum((jnp.sum(second_sum, 1), jnp.sum(second_sum * second_sum, 1)), '...  4.93 us
    all_to_all x1, starting transfers between devices, shards(): lax.all_to_all(summed.astype(jnp.bfloat16), 'ep', split_axis=0, concat_ax...  3.54 us
    dot_general x1, matrix products, time_mixer(): removed = jnp.einsum('bhij,bhj->bhi', state, -unit_keys)  3.51 us
  transfers between devices with their start and end apart: 4, of which 3 were waited for; matrix products, arithmetic and copies ran while one was open for 1% of the time, Pallas kernels for 0%

commit v1 on v0

--- a/solution.py
+++ b/solution.py
@@ -2,6 +2,7 @@
 import jax.numpy as jnp
 from jax import lax
 from jax.sharding import PartitionSpec as P
+from jax.lax import axis_index, axis_size, ppermute
 
 SPLIT = 4
 residual_scale = 1.4142135623730951
@@ -110,6 +111,22 @@
     routes,
     route_weights,
 ):
+
+    def _show_area(bus_axis, d_out, t0):
+        nodes = axis_size(bus_axis)
+        found = [t0]
+        it = 0
+        while it < nodes - 1:
+            found.append(
+                ppermute(found[-1], bus_axis, [(j, (j + 1) % nodes) for j in range(nodes)])
+            )
+            it += 1
+        return jnp.roll(
+            jnp.concatenate(found[::-1], d_out),
+            (axis_index(bus_axis) + 1) * t0.shape[d_out],
+            axis=d_out,
+        )
+
     row_count = tokens.shape[0]
     model_width = tokens.shape[1]
     quarter = w_recep.shape[1]
@@ -165,7 +182,7 @@
         preferred_element_type=jnp.float32,
     )
     branch = jax.nn.sigmoid(jnp.dot(x_mid, branch_gate, preferred_element_type=jnp.float32))
-    shard_rows = lax.all_gather(x_mid, "ep", axis=0, tiled=True)
+    shard_rows = _show_area("ep", 0, x_mid)
     gate_pre = lax.dot_general(
         shard_rows, dense_gate, (((1,), (1,)), ((), ())), preferred_element_type=jnp.float32
     )

time: 163 us -> 274 us (1.68)
  waiting for transfers between devices: 72.3 us -> 170 us
  local copies, waits for them, and re-layouts: 0.98 us -> 42.2 us
  blocking collectives: 45.9 us -> 4.93 us
  starting transfers between devices: 3.63 us -> 11.6 us
  matrix products: 21.3 us -> 24.8 us
    ppermute x0 -> x15, waiting for transfers between devices: none -> 84.2 us  [_show_area(): ppermute(found[-1], bus_axis, [(j, (j + 1) % nodes) for j in range(nodes)])]
    unnamed x29 -> x80, local copies, waits for them, and re-layouts: 0.09 us -> 39.9 us
    all_gather x1 -> x0, blocking collectives: 21.3 us -> none  [shards(): shard_rows = lax.all_gather(x_mid, 'ep', axis=0, tiled=True)]
    all_to_all x1 -> x0, blocking collectives: 19.7 us -> none  [shards(): lax.all_to_all(outgoing, 'ep', split_axis=0, concat_axis=0, tiled=True)]
    reduce_scatter x1, waiting for transfers between devices: 0.02 us -> 8.14 us  [shards(): lax.psum_scatter(partial_out.astype(jnp.bfloat16), 'tp', scatter_dimensio...]
    all_to_all x0 -> x1, starting transfers between devices: none -> 5.83 us  [shards(): lax.all_to_all(outgoing, 'ep', split_axis=0, concat_axis=0, tiled=True)]
    reduce_scatter x1, waiting for transfers between devices: 39.1 us -> 44.1 us  [shards(): lax.psum_scatter(jnp.dot(dense_hidden, dense_down, preferred_element_type...]
  transfers between devices with their start and end apart: 4 -> 20, of which waited for: 3 -> 18; matrix products, arithmetic and copies ran while one was open for 1% -> 16% of each run, Pallas kernels for 0% -> 0%
where the time goes in v1:
time: 274 us; the launch traced here: 272 us
  waiting for transfers between devices  170 us (62%)
  local copies, waits for them, and re-layouts  42.2 us (15%)
  matrix products  24.8 us (9%)
  between operations  13.5 us (5%)
  starting transfers between devices  11.6 us (4%)
  blocking collectives  4.93 us (2%)
  other arithmetic  4.44 us (2%)
    ppermute x15, waiting for transfers between devices, _show_area(): ppermute(found[-1], bus_axis, [(j, (j + 1) % nodes) for j in range(nodes)])  84.2 us
    reduce_scatter x1, waiting for transfers between devices, shards(): lax.psum_scatter(jnp.dot(dense_hidden, dense_down, preferred_element_type...  44.1 us
    unnamed x80, local copies, waits for them, and re-layouts  39.9 us
    psum x1, waiting for transfers between devices, shards(): mixed = lax.psum(partial_mix, 'tp')  23.8 us
    all_to_all x1, waiting for transfers between devices, shards(): lax.all_to_all(summed.astype(jnp.bfloat16), 'ep', split_axis=0, concat_ax...  9.77 us
    reduce_scatter x1, waiting for transfers between devices, shards(): lax.psum_scatter(partial_out.astype(jnp.bfloat16), 'tp', scatter_dimensio...  8.14 us
    all_to_all x1, starting transfers between devices, shards(): lax.all_to_all(outgoing, 'ep', split_axis=0, concat_axis=0, tiled=True)  5.83 us
    all_to_all x1, starting transfers between devices, shards(): lax.all_to_all(summed.astype(jnp.bfloat16), 'ep', split_axis=0, concat_ax...  5.62 us
  transfers between devices with their start and end apart: 20, of which 18 were waited for; matrix products, arithmetic and copies ran while one was open for 16% of the time, Pallas kernels for 0%

profile of v1, /device:TPU:0, one launch (start us, length us, event | category | flops | bytes accessed | tf_op | source)
XLA Modules:
  0.0 271.6 jit_solution(1051494662978393004)
XLA Ops:
  6.5 1.6 fusion.61
  9.6 1.5 fusion.64
  12.6 1.5 fusion.63
  14.2 3.5 %fusion.62 = f32[16,8,1,64]{3,2,1,0:T(1,128)S(1)} fusion(f32[16,8,64,1]{2,3,1,0:T(1,128)S(1)} %bitcast.78, f32[16,8,64,64]{3,2,1,0:T(8,128)} %param.25), kind=kOutput, calls=%fused_computation.117 | convolution fusion | flops 1048576 | bytes 2162688 | tf_op jit(solution)/shard_map/bhij,bhj->bhi/dot_general | solution.py:52
  17.8 2.9 %fusion = f32[16,8,1,64]{3,2,1,0:T(1,128)S(1)} fusion(f32[16,8,64,1]{2,3,1,0:T(1,128)S(1)} %bitcast.80, f32[16,8,64,64]{3,2,1,0:T(8,128)S(1)} %copy-done.1, f32[16,8,64]{2,1,0:T(8,128)S(1)} %reshape.96, f32[16,8,64]{2,1,0:T(8,128)S(1)} %mul.180, f32[16,8,64]{2,1,0:T(8,128)S(1)} %get-tuple-element.10, f32[16,8,64]{2,1,0:T(8,128)S(1)} %bitcast.79, ...), kind=kOutput, calls=%fused_computation | convolution fusion | flops 3670016 | bytes 2326528 | tf_op jit(solution)/shard_map/bhij,bhj->bhi/dot_general | solution.py:58
  21.2 2.1 fusion.53
  23.3 23.8 %all-reduce.3.cloned.1.call-done = f32[16,1024]{1,0:T(8,128)} async-done(((f32[16,1024]{1,0:T(8,128)}), f32[16,1024]{1,0:T(8,128)}) %all-reduce.3.cloned.1.call-update) | async-done | bytes 65552 | tf_op jit(solution)/shard_map/psum | solution.py:149
  50.2 6.0 %collective-permute-done = bf16[16,1024]{1,0:T(8,128)(2,1)S(1)} collective-permute-done((bf16[16,1024]{1,0:T(8,128)(2,1)S(1)}, bf16[16,1024]{1,0:T(8,128)(2,1)S(1)}, u32[]{:S(2)}, u32[]{:S(2)}) %collective-permute-start) | collective-permute-done | bytes 32800 | tf_op jit(solution)/shard_map/ppermute | solution.py:121
  56.2 6.0 %collective-permute-done.1 = bf16[16,1024]{1,0:T(8,128)(2,1)S(1)} collective-permute-done((bf16[16,1024]{1,0:T(8,128)(2,1)S(1)}, bf16[16,1024]{1,0:T(8,128)(2,1)S(1)}, u32[]{:S(2)}, u32[]{:S(2)}) %collective-permute-start.1) | collective-permute-done | bytes 32800 | tf_op jit(solution)/shard_map/ppermute | solution.py:121
  62.2 6.0 %collective-permute-done.2 = bf16[16,1024]{1,0:T(8,128)(2,1)S(1)} collective-permute-done((bf16[16,1024]{1,0:T(8,128)(2,1)S(1)}, bf16[16,1024]{1,0:T(8,128)(2,1)S(1)}, u32[]{:S(2)}, u32[]{:S(2)}) %collective-permute-start.2) | collective-permute-done | bytes 32800 | tf_op jit(solution)/shard_map/ppermute | solution.py:121
  68.3 6.0 %collective-permute-done.3 = bf16[16,1024]{1,0:T(8,128)(2,1)S(1)} collective-permute-done((bf16[16,1024]{1,0:T(8,128)(2,1)S(1)}, bf16[16,1024]{1,0:T(8,128)(2,1)S(1)}, u32[]{:S(2)}, u32[]{:S(2)}) %collective-permute-start.3) | collective-permute-done | bytes 32800 | tf_op jit(solution)/shard_map/ppermute | solution.py:121
  74.9 6.0 %collective-permute-done.4 = bf16[16,1024]{1,0:T(8,128)(2,1)S(1)} collective-permute-done((bf16[16,1024]{1,0:T(8,128)(2,1)S(1)}, bf16[16,1024]{1,0:T(8,128)(2,1)S(1)}, u32[]{:S(2)}, u32[]{:S(2)}) %collective-permute-start.4) | collective-permute-done | bytes 32800 | tf_op jit(solution)/shard_map/ppermute | solution.py:121
  81.6 6.0 %collective-permute-done.5 = bf16[16,1024]{1,0:T(8,128)(2,1)S(1)} collective-permute-done((bf16[16,1024]{1,0:T(8,128)(2,1)S(1)}, bf16[16,1024]{1,0:T(8,128)(2,1)S(1)}, u32[]{:S(2)}, u32[]{:S(2)}) %collective-permute-start.5) | collective-permute-done | bytes 32800 | tf_op jit(solution)/shard_map/ppermute | solution.py:121
  88.2 6.0 %collective-permute-done.6 = bf16[16,1024]{1,0:T(8,128)(2,1)S(1)} collective-permute-done((bf16[16,1024]{1,0:T(8,128)(2,1)S(1)}, bf16[16,1024]{1,0:T(8,128)(2,1)S(1)}, u32[]{:S(2)}, u32[]{:S(2)}) %collective-permute-start.6) | collective-permute-done | bytes 32800 | tf_op jit(solution)/shard_map/ppermute | solution.py:121
  94.8 6.0 %collective-permute-done.7 = bf16[16,1024]{1,0:T(8,128)(2,1)S(1)} collective-permute-done((bf16[16,1024]{1,0:T(8,128)(2,1)S(1)}, bf16[16,1024]{1,0:T(8,128)(2,1)S(1)}, u32[]{:S(2)}, u32[]{:S(2)}) %collective-permute-start.7) | collective-permute-done | bytes 32800 | tf_op jit(solution)/shard_map/ppermute | solution.py:121
  101.5 6.0 %collective-permute-done.8 = bf16[16,1024]{1,0:T(8,128)(2,1)S(1)} collective-permute-done((bf16[16,1024]{1,0:T(8,128)(2,1)S(1)}, bf16[16,1024]{1,0:T(8,128)(2,1)S(1)}, u32[]{:S(2)}, u32[]{:S(2)}) %collective-permute-start.8) | collective-permute-done | bytes 32800 | tf_op jit(solution)/shard_map/ppermute | solution.py:121
  108.1 6.0 %collective-permute-done.9 = bf16[16,1024]{1,0:T(8,128)(2,1)S(1)} collective-permute-done((bf16[16,1024]{1,0:T(8,128)(2,1)S(1)}, bf16[16,1024]{1,0:T(8,128)(2,1)S(1)}, u32[]{:S(2)}, u32[]{:S(2)}) %collective-permute-start.9) | collective-permute-done | bytes 32800 | tf_op jit(solution)/shard_map/ppermute | solution.py:121
  114.4 5.8 %collective-permute-done.10 = bf16[16,1024]{1,0:T(8,128)(2,1)S(1)} collective-permute-done((bf16[16,1024]{1,0:T(8,128)(2,1)S(1)}, bf16[16,1024]{1,0:T(8,128)(2,1)S(1)}, u32[]{:S(2)}, u32[]{:S(2)}) %collective-permute-start.10) | collective-permute-done | bytes 32800 | tf_op jit(solution)/shard_map/ppermute | solution.py:121
  120.2 6.0 %collective-permute-done.11 = bf16[16,1024]{1,0:T(8,128)(2,1)S(1)} collective-permute-done((bf16[16,1024]{1,0:T(8,128)(2,1)S(1)}, bf16[16,1024]{1,0:T(8,128)(2,1)S(1)}, u32[]{:S(2)}, u32[]{:S(2)}) %collective-permute-start.11) | collective-permute-done | bytes 32800 | tf_op jit(solution)/shard_map/ppermute | solution.py:121
  126.2 6.0 %collective-permute-done.12 = bf16[16,1024]{1,0:T(8,128)(2,1)S(1)} collective-permute-done((bf16[16,1024]{1,0:T(8,128)(2,1)S(1)}, bf16[16,1024]{1,0:T(8,128)(2,1)S(1)}, u32[]{:S(2)}, u32[]{:S(2)}) %collective-permute-start.12) | collective-permute-done | bytes 32800 | tf_op jit(solution)/shard_map/ppermute | solution.py:121
  132.3 6.1 %collective-permute-done.13 = bf16[16,1024]{1,0:T(8,128)(2,1)} collective-permute-done((bf16[16,1024]{1,0:T(8,128)(2,1)S(1)}, bf16[16,1024]{1,0:T(8,128)(2,1)}, u32[]{:S(2)}, u32[]{:S(2)}) %collective-permute-start.13) | collective-permute-done | bytes 32800 | tf_op jit(solution)/shard_map/ppermute | solution.py:121
  139.5 5.8 %all-to-all-start = ((bf16[16,16,1024]{2,1,0:T(8,128)(2,1)}), bf16[16,16,1024]{2,1,0:T(8,128)(2,1)S(1)}, u32[]{:S(2)}, u32[]{:S(2)}) async-start(bf16[16,16,1024]{2,1,0:T(8,128)(2,1)} %bitcast.8), calls=%async_computation | async-start | bytes 1048576 | tf_op jit(solution)/shard_map/all_to_all | solution.py:159
  145.4 1.4 constant_dynamic-update-slice_fusion.31
  148.1 1.4 constant_dynamic-update-slice_fusion.29
  149.5 1.4 constant_dynamic-update-slice_fusion.28
  150.9 1.4 constant_dynamic-update-slice_fusion.27
  153.6 1.4 constant_dynamic-update-slice_fusion.25
  155.0 1.4 constant_dynamic-update-slice_fusion.24
  156.3 1.4 constant_dynamic-update-slice_fusion.23
  157.7 1.4 constant_dynamic-update-slice_fusion.22
  159.1 1.4 constant_dynamic-update-slice_fusion.21
  160.4 1.4 constant_dynamic-update-slice_fusion.20
  164.2 1.4 constant_dynamic-update-slice_fusion.15
  165.6 1.4 constant_dynamic-update-slice_fusion.14
  166.9 1.4 constant_dynamic-update-slice_fusion.13
  173.7 1.4 constant_dynamic-update-slice_fusion.8
  175.1 1.4 constant_dynamic-update-slice_fusion.7
  176.4 1.4 constant_dynamic-update-slice_fusion.6
  177.8 1.4 constant_dynamic-update-slice_fusion.5
  179.8 2.0 fusion.23
  182.0 1.4 fusion.17
  186.5 1.4 fusion.37
  187.9 2.5 fusion.41
  190.5 8.1 %reduce-scatter.3.cloned.1.call-done = bf16[16,16,512]{2,1,0:T(8,128)(2,1)} async-done(((bf16[16,16,1024]{2,1,0:T(8,128)(2,1)}), bf16[16,16,512]{2,1,0:T(8,128)(2,1)}) %reduce-scatter.3.cloned.1.call-update) | async-done | bytes 262160 | tf_op jit(solution)/shard_map/reduce_scatter | solution.py:169
  198.6 5.6 %all-to-all-start.1 = ((bf16[16,16,512]{2,1,0:T(8,128)(2,1)}), bf16[16,16,512]{2,1,0:T(8,128)(2,1)S(1)}, u32[]{:S(2)}, u32[]{:S(2)}) async-start(bf16[16,16,512]{2,1,0:T(8,128)(2,1)} %reduce-scatter.3.cloned.1.call-done), calls=%async_computation.2 | async-start | bytes 524288 | tf_op jit(solution)/shard_map/all_to_all | solution.py:172
  204.5 9.8 %all-to-all-done.1 = bf16[16,16,512]{2,1,0:T(8,128)(2,1)S(1)} async-done(((bf16[16,16,512]{2,1,0:T(8,128)(2,1)}), bf16[16,16,512]{2,1,0:T(8,128)(2,1)S(1)}, u32[]{:S(2)}, u32[]{:S(2)}) %all-to-all-start.1) | async-done | bytes 262176 | tf_op jit(solution)/shard_map/all_to_all | solution.py:172
  214.3 44.1 %reduce-scatter.5.cloned.1.call-done = f32[16,512]{1,0:T(8,128)} async-done(((f32[256,512]{1,0:T(8,128)}), f32[16,512]{1,0:T(8,128)}) %reduce-scatter.5.cloned.1.call-update) | async-done | bytes 32784 | tf_op jit(solution)/shard_map/reduce_scatter | solution.py:193
  259.4 4.9 %all-reduce = (f32[16]{0:T(128)S(1)}, f32[16]{0:T(128)S(1)}) all-reduce(f32[16]{0:T(128)S(1)} %get-tuple-element.6, f32[16]{0:T(128)S(1)} %get-tuple-element.5), channel_id=1, replica_groups=mesh['ep'=16,'tp'=2] {'tp'}, use_global_device_ids=true, to_apply=%region_17.18 | all-reduce | flops 32 | bytes 256 | tf_op jit(solution)/shard_map/psum | solution.py:204
  (126 shorter events, 28.2 us)
Async XLA Ops:
  6.5 175.5 %copy-start = (bf16[1,704,1024]{2,1,0:T(8,128)(2,1)S(1)}, bf16[1,704,1024]{2,1,0:T(8,128)(2,1)}, u32[]{:S(2)}) copy-start(bf16[1,704,1024]{2,1,0:T(8,128)(2,1)} %param.40) | copy-start | bytes 4325380
  6.5 40.6 %all-reduce.3.cloned.1.call-start = ((), (), s32[]{:S(2)}) async-start(), calls=%async_computation.4 | async-start | bytes 131072 | tf_op jit(solution)/shard_map/psum | solution.py:149
  14.1 3.6 %copy-start.1 = (f32[16,8,64,64]{3,2,1,0:T(8,128)S(1)}, f32[16,8,64,64]{3,2,1,0:T(8,128)}, u32[]{:S(2)}) copy-start(f32[16,8,64,64]{3,2,1,0:T(8,128)} %param.25) | copy-start | bytes 6291460
  17.7 3.5 %copy-start.18 = (f32[512]{0:T(512)S(1)}, f32[512]{0:T(512)}, u32[]{:S(2)}) copy-start(f32[512]{0:T(512)} %param.36) | copy-start | bytes 6148
  17.7 29.4 %copy-start.2 = (bf16[16,1024]{1,0:T(8,128)(2,1)S(1)}, bf16[16,1024]{1,0:T(8,128)(2,1)}, u32[]{:S(2)}) copy-start(bf16[16,1024]{1,0:T(8,128)(2,1)} %param.24) | copy-start | bytes 98308
  17.7 31.4 %copy-start.17 = (f32[1024]{0:T(1024)S(1)}, f32[1024]{0:T(1024)}, u32[]{:S(2)}) copy-start(f32[1024]{0:T(1024)} %param.37) | copy-start | bytes 12292
  17.8 96.4 %copy-start.16 = (s32[16,2]{0,1:T(2,128)S(1)}, s32[16,2]{0,1:T(2,128)}, u32[]{:S(2)}) copy-start(s32[16,2]{0,1:T(2,128)} %param.46) | copy-start | bytes 388
  20.7 158.4 %copy-start.3 = (bf16[1,1024,704]{1,2,0:T(8,128)(2,1)S(1)}, bf16[1,1024,704]{1,2,0:T(8,128)(2,1)}, u32[]{:S(2)}) copy-start(bf16[1,1024,704]{1,2,0:T(8,128)(2,1)} %param.38) | copy-start | bytes 4325380
  50.1 6.1 %collective-permute-start = (bf16[16,1024]{1,0:T(8,128)(2,1)S(1)}, bf16[16,1024]{1,0:T(8,128)(2,1)S(1)}, u32[]{:S(2)}, u32[]{:S(2)}) collective-permute-start(bf16[16,1024]{1,0:T(8,128)(2,1)S(1)} %multiply_convert_fusion.2), channel_id=1, source_target_pairs={{0,2},{2,4},{4,6},{6,8},{8,10},{10,12},{12,14},{14,16},{16,18},{18... | collective-permute-start | bytes 98312 | tf_op jit(solution)/shard_map/ppermute | solution.py:121
  56.2 6.0 %collective-permute-start.1 = (bf16[16,1024]{1,0:T(8,128)(2,1)S(1)}, bf16[16,1024]{1,0:T(8,128)(2,1)S(1)}, u32[]{:S(2)}, u32[]{:S(2)}) collective-permute-start(bf16[16,1024]{1,0:T(8,128)(2,1)S(1)} %collective-permute-done), channel_id=1, source_target_pairs={{0,2},{2,4},{4,6},{6,8},{8,10},{10,12},{12,14},{14,16},{16,18},{18... | collective-permute-start | bytes 98312 | tf_op jit(solution)/shard_map/ppermute | solution.py:121
  62.2 6.0 %collective-permute-start.2 = (bf16[16,1024]{1,0:T(8,128)(2,1)S(1)}, bf16[16,1024]{1,0:T(8,128)(2,1)S(1)}, u32[]{:S(2)}, u32[]{:S(2)}) collective-permute-start(bf16[16,1024]{1,0:T(8,128)(2,1)S(1)} %collective-permute-done.1), channel_id=1, source_target_pairs={{0,2},{2,4},{4,6},{6,8},{8,10},{10,12},{12,14},{14,16},{16,18},{18... | collective-permute-start | bytes 98312 | tf_op jit(solution)/shard_map/ppermute | solution.py:121
  68.3 6.0 %collective-permute-start.3 = (bf16[16,1024]{1,0:T(8,128)(2,1)S(1)}, bf16[16,1024]{1,0:T(8,128)(2,1)S(1)}, u32[]{:S(2)}, u32[]{:S(2)}) collective-permute-start(bf16[16,1024]{1,0:T(8,128)(2,1)S(1)} %collective-permute-done.2), channel_id=1, source_target_pairs={{0,2},{2,4},{4,6},{6,8},{8,10},{10,12},{12,14},{14,16},{16,18},{18... | collective-permute-start | bytes 98312 | tf_op jit(solution)/shard_map/ppermute | solution.py:121
  74.3 0.6 copy-start.5
  74.9 6.0 %collective-permute-start.4 = (bf16[16,1024]{1,0:T(8,128)(2,1)S(1)}, bf16[16,1024]{1,0:T(8,128)(2,1)S(1)}, u32[]{:S(2)}, u32[]{:S(2)}) collective-permute-start(bf16[16,1024]{1,0:T(8,128)(2,1)S(1)} %collective-permute-done.3), channel_id=1, source_target_pairs={{0,2},{2,4},{4,6},{6,8},{8,10},{10,12},{12,14},{14,16},{16,18},{18... | collective-permute-start | bytes 98312 | tf_op jit(solution)/shard_map/ppermute | solution.py:121
  80.9 0.6 copy-start.7
  81.5 6.0 %collective-permute-start.5 = (bf16[16,1024]{1,0:T(8,128)(2,1)S(1)}, bf16[16,1024]{1,0:T(8,128)(2,1)S(1)}, u32[]{:S(2)}, u32[]{:S(2)}) collective-permute-start(bf16[16,1024]{1,0:T(8,128)(2,1)S(1)} %collective-permute-done.4), channel_id=1, source_target_pairs={{0,2},{2,4},{4,6},{6,8},{8,10},{10,12},{12,14},{14,16},{16,18},{18... | collective-permute-start | bytes 98312 | tf_op jit(solution)/shard_map/ppermute | solution.py:121
  87.6 0.6 copy-start.8
  88.2 6.0 %collective-permute-start.6 = (bf16[16,1024]{1,0:T(8,128)(2,1)S(1)}, bf16[16,1024]{1,0:T(8,128)(2,1)S(1)}, u32[]{:S(2)}, u32[]{:S(2)}) collective-permute-start(bf16[16,1024]{1,0:T(8,128)(2,1)S(1)} %collective-permute-done.5), channel_id=1, source_target_pairs={{0,2},{2,4},{4,6},{6,8},{8,10},{10,12},{12,14},{14,16},{16,18},{18... | collective-permute-start | bytes 98312 | tf_op jit(solution)/shard_map/ppermute | solution.py:121
  94.2 0.6 copy-start.9
  94.8 6.0 %collective-permute-start.7 = (bf16[16,1024]{1,0:T(8,128)(2,1)S(1)}, bf16[16,1024]{1,0:T(8,128)(2,1)S(1)}, u32[]{:S(2)}, u32[]{:S(2)}) collective-permute-start(bf16[16,1024]{1,0:T(8,128)(2,1)S(1)} %collective-permute-done.6), channel_id=1, source_target_pairs={{0,2},{2,4},{4,6},{6,8},{8,10},{10,12},{12,14},{14,16},{16,18},{18... | collective-permute-start | bytes 98312 | tf_op jit(solution)/shard_map/ppermute | solution.py:121
  100.9 0.6 copy-start.10
  101.5 6.0 %collective-permute-start.8 = (bf16[16,1024]{1,0:T(8,128)(2,1)S(1)}, bf16[16,1024]{1,0:T(8,128)(2,1)S(1)}, u32[]{:S(2)}, u32[]{:S(2)}) collective-permute-start(bf16[16,1024]{1,0:T(8,128)(2,1)S(1)} %collective-permute-done.7), channel_id=1, source_target_pairs={{0,2},{2,4},{4,6},{6,8},{8,10},{10,12},{12,14},{14,16},{16,18},{18... | collective-permute-start | bytes 98312 | tf_op jit(solution)/shard_map/ppermute | solution.py:121
  107.5 0.6 copy-start.11
  108.1 6.0 %collective-permute-start.9 = (bf16[16,1024]{1,0:T(8,128)(2,1)S(1)}, bf16[16,1024]{1,0:T(8,128)(2,1)S(1)}, u32[]{:S(2)}, u32[]{:S(2)}) collective-permute-start(bf16[16,1024]{1,0:T(8,128)(2,1)S(1)} %collective-permute-done.8), channel_id=1, source_target_pairs={{0,2},{2,4},{4,6},{6,8},{8,10},{10,12},{12,14},{14,16},{16,18},{18... | collective-permute-start | bytes 98312 | tf_op jit(solution)/shard_map/ppermute | solution.py:121
  114.1 25.4 %copy-start.12 = (bf16[16,1024]{1,0:T(8,128)(2,1)}, bf16[16,1024]{1,0:T(8,128)(2,1)S(1)}, u32[]{:S(2)}) copy-start(bf16[16,1024]{1,0:T(8,128)(2,1)S(1)} %collective-permute-done.9) | copy-start | bytes 98308
  114.1 6.0 %collective-permute-start.10 = (bf16[16,1024]{1,0:T(8,128)(2,1)S(1)}, bf16[16,1024]{1,0:T(8,128)(2,1)S(1)}, u32[]{:S(2)}, u32[]{:S(2)}) collective-permute-start(bf16[16,1024]{1,0:T(8,128)(2,1)S(1)} %collective-permute-done.9), channel_id=1, source_target_pairs={{0,2},{2,4},{4,6},{6,8},{8,10},{10,12},{12,14},{14,16},{16,18},{18... | collective-permute-start | bytes 98312 | tf_op jit(solution)/shard_map/ppermute | solution.py:121
  120.2 19.3 %copy-start.13 = (bf16[16,1024]{1,0:T(8,128)(2,1)}, bf16[16,1024]{1,0:T(8,128)(2,1)S(1)}, u32[]{:S(2)}) copy-start(bf16[16,1024]{1,0:T(8,128)(2,1)S(1)} %collective-permute-done.10) | copy-start | bytes 98308
  120.2 6.0 %collective-permute-start.11 = (bf16[16,1024]{1,0:T(8,128)(2,1)S(1)}, bf16[16,1024]{1,0:T(8,128)(2,1)S(1)}, u32[]{:S(2)}, u32[]{:S(2)}) collective-permute-start(bf16[16,1024]{1,0:T(8,128)(2,1)S(1)} %collective-permute-done.10), channel_id=1, source_target_pairs={{0,2},{2,4},{4,6},{6,8},{8,10},{10,12},{12,14},{14,16},{16,18},{18... | collective-permute-start | bytes 98312 | tf_op jit(solution)/shard_map/ppermute | solution.py:121
  126.2 13.3 %copy-start.14 = (bf16[16,1024]{1,0:T(8,128)(2,1)}, bf16[16,1024]{1,0:T(8,128)(2,1)S(1)}, u32[]{:S(2)}) copy-start(bf16[16,1024]{1,0:T(8,128)(2,1)S(1)} %collective-permute-done.11) | copy-start | bytes 98308
  126.2 6.0 %collective-permute-start.12 = (bf16[16,1024]{1,0:T(8,128)(2,1)S(1)}, bf16[16,1024]{1,0:T(8,128)(2,1)S(1)}, u32[]{:S(2)}, u32[]{:S(2)}) collective-permute-start(bf16[16,1024]{1,0:T(8,128)(2,1)S(1)} %collective-permute-done.11), channel_id=1, source_target_pairs={{0,2},{2,4},{4,6},{6,8},{8,10},{10,12},{12,14},{14,16},{16,18},{18... | collective-permute-start | bytes 98312 | tf_op jit(solution)/shard_map/ppermute | solution.py:121
  132.3 7.3 %copy-start.15 = (bf16[16,1024]{1,0:T(8,128)(2,1)}, bf16[16,1024]{1,0:T(8,128)(2,1)S(1)}, u32[]{:S(2)}) copy-start(bf16[16,1024]{1,0:T(8,128)(2,1)S(1)} %collective-permute-done.12) | copy-start | bytes 98308
  132.3 6.1 %collective-permute-start.13 = (bf16[16,1024]{1,0:T(8,128)(2,1)S(1)}, bf16[16,1024]{1,0:T(8,128)(2,1)}, u32[]{:S(2)}, u32[]{:S(2)}) collective-permute-start(bf16[16,1024]{1,0:T(8,128)(2,1)S(1)} %collective-permute-done.12), channel_id=1, source_target_pairs={{0,2},{2,4},{4,6},{6,8},{8,10},{10,12},{12,14},{14,16},{16,18},{18... | collective-permute-start | bytes 98312 | tf_op jit(solution)/shard_map/ppermute | solution.py:121
  138.4 7.0 %collective-permute-start.14 = (bf16[16,1024]{1,0:T(8,128)(2,1)}, bf16[16,1024]{1,0:T(8,128)(2,1)}, u32[]{:S(2)}, u32[]{:S(2)}) collective-permute-start(bf16[16,1024]{1,0:T(8,128)(2,1)} %collective-permute-done.13), channel_id=1, source_target_pairs={{0,2},{2,4},{4,6},{6,8},{8,10},{10,12},{12,14},{14,16},{16,18},{18... | collective-permute-start | bytes 98312 | tf_op jit(solution)/shard_map/ppermute | solution.py:121
  139.5 39.6 %all-to-all-start = ((bf16[16,16,1024]{2,1,0:T(8,128)(2,1)}), bf16[16,16,1024]{2,1,0:T(8,128)(2,1)S(1)}, u32[]{:S(2)}, u32[]{:S(2)}) async-start(bf16[16,16,1024]{2,1,0:T(8,128)(2,1)} %bitcast.8), calls=%async_computation | async-start | bytes 1048576 | tf_op jit(solution)/shard_map/all_to_all | solution.py:159
  145.4 53.3 %reduce-scatter.3.cloned.1.call-start = ((), (), s32[]{:S(2)}) async-start(), calls=%async_computation.5 | async-start | bytes 786432 | tf_op jit(solution)/shard_map/reduce_scatter | solution.py:169
  179.8 3.7 %copy-start.6 = (bf16[16,1024]{1,0:T(8,128)(2,1)S(1)}, bf16[16,1024]{1,0:T(8,128)(2,1)}, u32[]{:S(2)}) copy-start(bf16[16,1024]{1,0:T(8,128)(2,1)} %copy-done.5) | copy-start | bytes 98308
  179.8 6.8 %copy-start.4 = (bf16[176,1024]{1,0:T(8,128)(2,1)S(1)}, bf16[176,1024]{1,0:T(8,128)(2,1)}, u32[]{:S(2)}) copy-start(bf16[176,1024]{1,0:T(8,128)(2,1)} %param.42) | copy-start | bytes 1081348
  179.8 8.1 %copy-start.23 = (bf16[176,512]{1,0:T(8,128)(2,1)S(1)}, bf16[176,512]{1,0:T(8,128)(2,1)}, u32[]{:S(2)}) copy-start(bf16[176,512]{1,0:T(8,128)(2,1)} %param.43) | copy-start | bytes 540676
  181.8 6.1 %copy-start.22 = (bf16[176,1024]{1,0:T(8,128)(2,1)S(1)}, bf16[176,1024]{1,0:T(8,128)(2,1)}, u32[]{:S(2)}) copy-start(bf16[176,1024]{1,0:T(8,128)(2,1)} %param.41) | copy-start | bytes 1081348
  181.8 22.4 %copy-start.19 = (bf16[1024]{0:T(1024)(128)(2,1)S(1)}, bf16[1024]{0:T(1024)(128)(2,1)}, u32[]{:S(2)}) copy-start(bf16[1024]{0:T(1024)(128)(2,1)} %param.44) | copy-start | bytes 6148
  181.8 22.5 %copy-start.21 = (f32[16,2]{0,1:T(2,128)S(1)}, f32[16,2]{0,1:T(2,128)}, u32[]{:S(2)}) copy-start(f32[16,2]{0,1:T(2,128)} %param.47) | copy-start | bytes 388
  182.0 82.4 %copy-start.20 = (f32[512]{0:T(512)S(1)}, f32[512]{0:T(512)}, u32[]{:S(2)}) copy-start(f32[512]{0:T(512)} %param.45) | copy-start | bytes 6148
  183.4 74.9 %reduce-scatter.5.cloned.1.call-start = ((), (), s32[]{:S(2)}) async-start(), calls=%async_computation.6 | async-start | bytes 557056 | tf_op jit(solution)/shard_map/reduce_scatter | solution.py:193
  198.6 15.6 %all-to-all-start.1 = ((bf16[16,16,512]{2,1,0:T(8,128)(2,1)}), bf16[16,16,512]{2,1,0:T(8,128)(2,1)S(1)}, u32[]{:S(2)}, u32[]{:S(2)}) async-start(bf16[16,16,512]{2,1,0:T(8,128)(2,1)} %reduce-scatter.3.cloned.1.call-done), calls=%async_computation.2 | async-start | bytes 524288 | tf_op jit(solution)/shard_map/all_to_all | solution.py:172
Sparse Core Ops, SparseCore 0:
  23.4 23.6 all-reduce.2
  183.6 15.0 reduce-scatter.2
  202.2 56.1 reduce-scatter.4
